TPU v7x, 32 devices: a whole 2x2x4 slice. The times are simulated.
32 devices in a mesh: grp: 2 (over x), ep: 16 (over z, y, core).
Axes of the slice: x: 2, y: 2, z: 4, core: 2. Of those that a mesh axis runs over, the one named last changes fastest.
Arguments:
- tokens: bfloat16 [128, 2048], P(('grp', 'ep')), parts along dimension 0, may hold values from -30 to 30
- state: float32 [128, 16, 128, 128], P(('grp', 'ep')), parts along dimension 0, may hold values from -6 to 6
- route_ids: int32 [128, 2], P(('grp', 'ep')), parts along dimension 0, may hold values from 0 to 3, all different within a row; in each aligned block of 4 rows (0 to 3, 4 to 7, ...) at most 3 rows name the same one
- route_weights: bfloat16 [128, 2], P(('grp', 'ep')), parts along dimension 0, may hold values from 0.099609375 to 1
- norm_mix: float32 [2048], replicated, may hold values from 0.1 to 1.9
- w_query: bfloat16 [2048, 2048], P(None, 'ep'), may hold values from -0.125 to 0.125
- w_forget: bfloat16 [2048, 2048], P(None, 'ep'), may hold values from -0.125 to 0.125
- w_input: bfloat16 [2048, 2048], P(None, 'ep'), may hold values from -0.125 to 0.125
- w_gate: bfloat16 [2048, 2048], P(None, 'ep'), may hold values from -0.125 to 0.125
- lower_bound: float32 [2048], replicated, may hold values from 0.05 to 0.9
- head_gain: float32 [128], replicated, may hold values from 0.1 to 1.9
- w_out: bfloat16 [2048, 2048], P(None, 'ep'), may hold values from -0.125 to 0.125
- norm_ffn: float32 [2048], replicated, may hold values from 0.1 to 1.9
- expert_gate: bfloat16 [2048, 28672], P(None, 'ep'), may hold values from -0.125 to 0.125
- expert_up: bfloat16 [2048, 28672], P(None, 'ep'), may hold values from -0.125 to 0.125
- expert_down: bfloat16 [28672, 2048], P('ep'), may hold values from -0.0625 to 0.0625
Outputs:
- layer_out: bfloat16 [128, 2048], P(('grp', 'ep')), parts along dimension 0
- new_state: float32 [128, 16, 128, 128], P(('grp', 'ep')), parts along dimension 0
There are 2 independent parts, one for each index of `grp`. A program takes and returns all parts, laid end to end along the dimension named above; an argument that names none is the same for every part. Nothing has to cross between parts.
Inputs may be any that keep to these rules, and one draw needn't show every extreme that they name: `route_ids`: each row names 2 different experts; the rows of one device name no expert more than 3 times, and some device names one exactly 3 times.
All inputs are finite; a program needn't handle non-finite values.
Results may differ from a plain program's by a relative error of at most 0.008.
Values may be sent and summed in bfloat16 or wider, within the bound.
No kernel may reach another device: no remote copies, remote signals or barrier semaphores. Data moves between devices by JAX's collectives and lax.ppermute only.
A program may use at most 64 MiB of HBM per device.

v0:
```python
import jax
import jax.numpy as jnp
from jax import lax
from jax.sharding import PartitionSpec as P

FF = 7168
EXPERTS = 4
CAP = 3
epsilon = 1e-06


def rms_scale(values, gain):
    return values * lax.rsqrt(jnp.mean(values * values, axis=-1, keepdims=True) + epsilon) * gain


def mixer_state(projected, state, lower_bound, head_gain):
    query_raw = projected[0].astype(jnp.float32)
    forget_raw = projected[1].astype(jnp.float32)
    input_raw = projected[2].astype(jnp.float32)
    gate_raw = projected[3].astype(jnp.float32)
    seq_rows = state.shape[0]
    heads = state.shape[1]
    head_dim = state.shape[2]
    head_shape = (seq_rows, heads, head_dim)
    log_forget = jnp.logaddexp(
        jnp.log(lower_bound), jnp.log1p(-lower_bound) + jax.nn.log_sigmoid(forget_raw)
    )
    key_vec = (1.0 - lower_bound) * jax.nn.sigmoid(-forget_raw)
    query_vec = jax.nn.silu(query_raw) * head_dim ** (-0.5)
    new_state = (
        jnp.exp(log_forget).reshape(head_shape)[..., None] * state
        + key_vec.reshape(head_shape)[..., None] * input_raw.reshape(head_shape)[:, :, None, :]
    )
    read_out = jnp.einsum(
        "thk,thkv->thv", query_vec.reshape(head_shape), new_state, precision=lax.Precision.HIGHEST
    )
    mixed = rms_scale(read_out, head_gain) * jax.nn.silu(gate_raw.reshape(head_shape))
    return (mixed.reshape(seq_rows, heads * head_dim).astype(jnp.bfloat16), new_state)


def local(
    tokens,
    state,
    route_ids,
    route_weights,
    norm_mix,
    w_query,
    w_forget,
    w_input,
    w_gate,
    lower_bound,
    head_gain,
    w_out,
    norm_ffn,
    expert_gate,
    expert_up,
    expert_down,
):
    model_width = tokens.shape[1]
    expert_group = FF // expert_gate.shape[1]
    all_tokens, all_ids, all_weights = (
        lax.all_gather(tokens, "ep", axis=0, tiled=True),
        lax.all_gather(route_ids, "ep", axis=0, tiled=True),
        lax.all_gather(route_weights, "ep", axis=0, tiled=True),
    )
    normed = rms_scale(all_tokens.astype(jnp.float32), norm_mix).astype(jnp.bfloat16)
    projected = jnp.stack(
        [
            jnp.dot(normed, weight, preferred_element_type=jnp.float32).astype(jnp.bfloat16)
            for weight in (w_query, w_forget, w_input, w_gate)
        ]
    )
    owned = lax.all_to_all(projected, "ep", split_axis=1, concat_axis=2, tiled=True)
    mixed, new_state = mixer_state(owned, state, lower_bound, head_gain)
    mixer_cols = jnp.dot(
        lax.all_gather(mixed, "ep", axis=0, tiled=True), w_out, preferred_element_type=jnp.float32
    ).astype(jnp.bfloat16)
    mixer_rows = lax.all_to_all(mixer_cols, "ep", split_axis=0, concat_axis=1, tiled=True)
    middle = tokens.astype(jnp.float32) + mixer_rows.astype(jnp.float32)
    normed_two = rms_scale(middle, norm_ffn).astype(jnp.bfloat16)
    matches = (route_ids[:, :, None] == jnp.arange(EXPERTS, dtype=jnp.int32)[None, None, :]).astype(
        jnp.int32
    )
    hit_mask = jnp.sum(matches, axis=1)
    combined = jnp.sum(
        route_weights.astype(jnp.float32)[:, :, None] * matches.astype(jnp.float32), axis=1
    )
    slot_rank = jnp.cumsum(hit_mask, axis=0) - hit_mask
    slot_ids = jnp.arange(CAP, dtype=jnp.int32)
    placing = (
        (slot_rank.T[:, None, :] == slot_ids[None, :, None]) & (hit_mask.T[:, None, :] > 0)
    ).astype(jnp.float32)
    outgoing = jnp.einsum(
        "ect,td->ecd", placing.astype(jnp.bfloat16), normed_two, preferred_element_type=jnp.float32
    ).astype(jnp.bfloat16)
    outgoing = jnp.repeat(outgoing, expert_group, axis=0)
    arrived = lax.all_to_all(outgoing, "ep", split_axis=0, concat_axis=0, tiled=True)
    gate_act = jnp.einsum("scd,df->scf", arrived, expert_gate, preferred_element_type=jnp.float32)
    up_act = jnp.einsum("scd,df->scf", arrived, expert_up, preferred_element_type=jnp.float32)
    hidden = (jax.nn.silu(gate_act) * up_act).astype(jnp.bfloat16)
    partial_rows = jnp.einsum(
        "scf,fd->scd", hidden, expert_down, preferred_element_type=jnp.float32
    )
    returned = lax.all_to_all(
        partial_rows.astype(jnp.bfloat16), "ep", split_axis=0, concat_axis=0, tiled=True
    ).astype(partial_rows.dtype)
    summed = jnp.sum(
        returned.reshape(EXPERTS, expert_group, returned.shape[1], model_width), axis=1
    )
    expert_total = jnp.einsum(
        "ect,ecd->td", placing * combined.T[:, None, :], summed, precision=lax.Precision.HIGHEST
    )
    layer_out = (middle + expert_total).astype(jnp.bfloat16)
    return (layer_out, new_state)


def solution(mesh):
    return jax.shard_map(
        local,
        mesh=mesh,
        in_specs=(
            P(("grp", "ep"), None),
            P(("grp", "ep"), None, None, None),
            P(("grp", "ep"), None),
            P(("grp", "ep"), None),
            P(),
            P(None, "ep"),
            P(None, "ep"),
            P(None, "ep"),
            P(None, "ep"),
            P(),
            P(),
            P(None, "ep"),
            P(),
            P(None, "ep"),
            P(None, "ep"),
            P("ep", None),
        ),
        out_specs=(P(("grp", "ep"), None), P(("grp", "ep"), None, None, None)),
        check_vma=False,
    )
```

profile of v0, /device:TPU:0, one launch (start us, length us, event | category | flops | bytes accessed | tf_op | source)
XLA Modules:
  0.0 121.8 jit_solution(15939425539012757206)
XLA Ops:
  0.6 24.2 %all-gather = bf16[16,4,2048]{2,1,0:T(4,128)(2,1)S(1)} all-gather(bf16[1,4,2048]{2,1,0:T(4,128)(2,1)} %bitcast.138), channel_id=1, replica_groups=mesh['grp'=2,'ep'=16] {'ep'}, dimensions={0}, use_global_device_ids=true | all-gather | bytes 278528 | tf_op jit(solution)/shard_map/all_gather | solution.py:62
  24.9 0.1 multiply_reduce_fusion
  25.0 0.8 multiply_convert_fusion
  25.9 0.2 fusion.17
  26.1 1.3 %fusion.18 = bf16[1,64,128]{2,1,0:T(8,128)(2,1)S(1)} fusion(bf16[64,2048]{1,0:T(8,128)(2,1)S(1)} %multiply_convert_fusion, bf16[2048,128]{1,0:T(8,128)(2,1)} %param.22), kind=kOutput, calls=%fused_computation.20 | convolution fusion | flops 33562624 | bytes 802816 | tf_op jit(solution)/shard_map/dot_general | solution.py:69
  27.4 1.3 %fusion.19 = bf16[1,64,128]{2,1,0:T(8,128)(2,1)S(1)} fusion(bf16[64,2048]{1,0:T(8,128)(2,1)S(1)} %multiply_convert_fusion, bf16[2048,128]{1,0:T(8,128)(2,1)} %param.23), kind=kOutput, calls=%fused_computation.21 | convolution fusion | flops 33562624 | bytes 802816 | tf_op jit(solution)/shard_map/dot_general | solution.py:69
  28.7 1.3 %fusion.20 = bf16[1,64,128]{2,1,0:T(8,128)(2,1)S(1)} fusion(bf16[64,2048]{1,0:T(8,128)(2,1)S(1)} %multiply_convert_fusion, bf16[2048,128]{1,0:T(8,128)(2,1)} %param.24), kind=kOutput, calls=%fused_computation.22 | convolution fusion | flops 33562624 | bytes 802816 | tf_op jit(solution)/shard_map/dot_general | solution.py:69
  30.0 0.7 copy.66
  30.7 3.5 %all-to-all-start = ((bf16[4,64,128]{2,0,1:T(4,128)(2,1)}), bf16[4,64,128]{2,0,1:T(4,128)(2,1)S(1)}, u32[]{:S(2)}, u32[]{:S(2)}) async-start(bf16[4,64,128]{2,0,1:T(4,128)(2,1)} %copy.66), calls=%async_computation | async-start | bytes 131072 | tf_op jit(solution)/shard_map/all_to_all | solution.py:73
  34.2 0.7 log_bitcast_fusion
  34.9 0.8 convert_reduce_fusion.1
  35.7 5.3 %all-to-all-done = bf16[4,64,128]{2,0,1:T(4,128)(2,1)S(1)} async-done(((bf16[4,64,128]{2,0,1:T(4,128)(2,1)}), bf16[4,64,128]{2,0,1:T(4,128)(2,1)S(1)}, u32[]{:S(2)}, u32[]{:S(2)}) %all-to-all-start) | async-done | bytes 65568 | tf_op jit(solution)/shard_map/all_to_all | solution.py:73
  41.2 4.4 %multiply_add_fusion = f32[4,16,128,128]{3,2,1,0:T(8,128)S(1)} fusion(f32[4,16,128,128]{3,2,1,0:T(8,128)} %param.17, f32[4,16,128]{2,1,0:T(8,128)S(1)} %fusion.57, f32[4,16,128]{2,1,0:T(8,128)S(1)} %get-tuple-element.3, f32[4,16,128]{2,1,0:T(8,128)S(1)} %get-tuple-element.2), kind=kLoop, calls=%fused_computation.6 | loop fusion | flops 3145728 | bytes 8486912 | tf_op jit(solution)/shard_map/add | solution.py:31
  45.6 2.0 %copy-done.1 = f32[4,16,128,128]{3,2,1,0:T(8,128)} copy-done((f32[4,16,128,128]{3,2,1,0:T(8,128)}, f32[4,16,128,128]{3,2,1,0:T(8,128)S(1)}, u32[]{:S(2)}) %copy-start.1) | copy-done | bytes 4194328
  47.6 3.6 %fusion.73 = f32[4,16,1,128]{3,2,1,0:T(1,128)S(1)} fusion(f32[4,16,128,1]{2,3,1,0:T(1,128)S(1)} %bitcast.137, f32[4,16,128,128]{3,2,1,0:T(8,128)S(1)} %multiply_add_fusion), kind=kOutput, calls=%fused_computation.103 | convolution fusion | flops 12582912 | bytes 4259840 | tf_op jit(solution)/shard_map/thk,thkv->thv/dot_general | solution.py:34
  51.3 0.1 multiply_reduce_fusion.2
  51.5 18.4 %all-gather.1 = bf16[16,4,2048]{2,1,0:T(4,128)(2,1)S(1)} all-gather(bf16[1,4,2048]{2,1,0:T(4,128)(2,1)S(1)} %reshape.164), channel_id=1, replica_groups=mesh['grp'=2,'ep'=16] {'ep'}, dimensions={0}, use_global_device_ids=true | all-gather | bytes 278528 | tf_op jit(solution)/shard_map/all_gather | solution.py:76
  70.0 0.8 convolution_convert_fusion.1
  70.8 3.5 %all-to-all-start.1 = ((bf16[16,4,128]{2,1,0:T(4,128)(2,1)}), bf16[16,4,128]{2,1,0:T(4,128)(2,1)S(1)}, u32[]{:S(2)}, u32[]{:S(2)}) async-start(bf16[16,4,128]{2,1,0:T(4,128)(2,1)} %bitcast.21), calls=%async_computation.1 | async-start | bytes 32768 | tf_op jit(solution)/shard_map/all_to_all | solution.py:78
  74.3 6.5 %all-to-all-done.1 = bf16[16,4,128]{2,1,0:T(4,128)(2,1)S(1)} async-done(((bf16[16,4,128]{2,1,0:T(4,128)(2,1)}), bf16[16,4,128]{2,1,0:T(4,128)(2,1)S(1)}, u32[]{:S(2)}, u32[]{:S(2)}) %all-to-all-start.1) | async-done | bytes 16416 | tf_op jit(solution)/shard_map/all_to_all | solution.py:78
  80.8 0.1 multiply_reduce_fusion.1
  80.9 0.2 convolution_convert_fusion
  81.2 0.1 broadcast_in_dim.2
  81.3 12.6 %all_to_all.38 = bf16[16,3,2048]{2,1,0:T(4,128)(2,1)S(1)} all-to-all(bf16[16,3,2048]{2,1,0:T(4,128)(2,1)S(1)} %bitcast.130), channel_id=1, replica_groups=mesh['grp'=2,'ep'=16] {'ep'}, dimensions={0} | all-to-all | bytes 393216 | tf_op jit(solution)/shard_map/all_to_all | solution.py:97
  93.9 4.5 %fusion.4 = f32[16,3,1792]{2,0,1:T(8,128)S(1)} fusion(bf16[2048,1792]{1,0:T(8,128)(2,1)} %param.29, bf16[16,3,2048]{2,1,0:T(4,128)(2,1)S(1)} %all_to_all.38), kind=kOutput, calls=%fused_computation.4 | convolution fusion | flops 352321536 | bytes 7880704 | tf_op jit(solution)/shard_map/scd,df->scf/dot_general | solution.py:98
  98.5 7.9 %fusion.12 = bf16[16,3,2048]{2,0,1:T(8,128)(2,1)S(1)} fusion(bf16[1792,2048]{1,0:T(8,128)(2,1)} %param.31, bf16[2048,1792]{1,0:T(8,128)(2,1)} %param.30, f32[16,3,1792]{2,0,1:T(8,128)S(1)} %fusion.4, bf16[16,3,2048]{2,1,0:T(4,128)(2,1)S(1)} %all_to_all.38), kind=kOutput, calls=%fused_computation.9 | convolution fusion | flops 705257472 | bytes 15417344 | tf_op jit(solution)/shard_map/scf,fd->scd/dot_general | solution.py:101
  106.4 0.9 copy.73
  107.2 3.5 %all-to-all-start.3 = ((bf16[16,3,2048]{2,1,0:T(4,128)(2,1)}), bf16[16,3,2048]{2,1,0:T(4,128)(2,1)S(1)}, u32[]{:S(2)}, u32[]{:S(2)}) async-start(bf16[16,3,2048]{2,1,0:T(4,128)(2,1)} %copy.73), calls=%async_computation.3 | async-start | bytes 524288 | tf_op jit(solution)/shard_map/all_to_all | solution.py:104
  110.8 0.1 fusion.63
  110.9 9.9 %all-to-all-done.3 = bf16[16,3,2048]{2,1,0:T(4,128)(2,1)S(1)} async-done(((bf16[16,3,2048]{2,1,0:T(4,128)(2,1)}), bf16[16,3,2048]{2,1,0:T(4,128)(2,1)S(1)}, u32[]{:S(2)}, u32[]{:S(2)}) %all-to-all-start.3) | async-done | bytes 196640 | tf_op jit(solution)/shard_map/all_to_all | solution.py:104
  120.7 0.1 convert_reduce_fusion
  120.9 0.9 fusion.16
  (31 shorter events, 0.5 us)
Async XLA Ops:
  0.6 25.2 %copy-start = (bf16[2048,128]{1,0:T(8,128)(2,1)S(1)}, bf16[2048,128]{1,0:T(8,128)(2,1)}, u32[]{:S(2)}) copy-start(bf16[2048,128]{1,0:T(8,128)(2,1)} %param.21) | copy-start | bytes 1572868
  28.7 22.7 %copy-start.5 = (f32[128]{0:T(128)S(1)}, f32[128]{0:T(128)}, u32[]{:S(2)}) copy-start(f32[128]{0:T(128)} %param.26) | copy-start | bytes 1540
  30.0 40.0 %copy-start.2 = (bf16[2048,128]{1,0:T(8,128)(2,1)S(1)}, bf16[2048,128]{1,0:T(8,128)(2,1)}, u32[]{:S(2)}) copy-start(bf16[2048,128]{1,0:T(8,128)(2,1)} %param.27) | copy-start | bytes 1572868
  30.7 10.4 %all-to-all-start = ((bf16[4,64,128]{2,0,1:T(4,128)(2,1)}), bf16[4,64,128]{2,0,1:T(4,128)(2,1)S(1)}, u32[]{:S(2)}, u32[]{:S(2)}) async-start(bf16[4,64,128]{2,0,1:T(4,128)(2,1)} %copy.66), calls=%async_computation | async-start | bytes 131072 | tf_op jit(solution)/shard_map/all_to_all | solution.py:73
  41.1 39.7 %copy-start.3 = (bf16[4,2048]{1,0:T(4,128)(2,1)S(1)}, bf16[4,2048]{1,0:T(4,128)(2,1)}, u32[]{:S(2)}) copy-start(bf16[4,2048]{1,0:T(4,128)(2,1)} %param.16) | copy-start | bytes 49156
  41.1 39.8 %copy-start.6 = (f32[2048]{0:T(1024)S(1)}, f32[2048]{0:T(1024)}, u32[]{:S(2)}) copy-start(f32[2048]{0:T(1024)} %param.28) | copy-start | bytes 24580
  45.6 2.0 %copy-start.1 = (f32[4,16,128,128]{3,2,1,0:T(8,128)}, f32[4,16,128,128]{3,2,1,0:T(8,128)S(1)}, u32[]{:S(2)}) copy-start(f32[4,16,128,128]{3,2,1,0:T(8,128)S(1)} %multiply_add_fusion) | copy-start | bytes 12582916
  70.8 10.0 %all-to-all-start.1 = ((bf16[16,4,128]{2,1,0:T(4,128)(2,1)}), bf16[16,4,128]{2,1,0:T(4,128)(2,1)S(1)}, u32[]{:S(2)}, u32[]{:S(2)}) async-start(bf16[16,4,128]{2,1,0:T(4,128)(2,1)} %bitcast.21), calls=%async_computation.1 | async-start | bytes 32768 | tf_op jit(solution)/shard_map/all_to_all | solution.py:78
  98.4 12.3 %copy-start.7 = (bf16[4,2]{0,1:T(2,128)(2,1)S(1)}, bf16[4,2]{0,1:T(2,128)(2,1)}, u32[]{:S(2)}) copy-start(bf16[4,2]{0,1:T(2,128)(2,1)} %param.19) | copy-start | bytes 52
  98.5 12.3 %copy-start.4 = (s32[4,2]{0,1:T(2,128)S(1)}, s32[4,2]{0,1:T(2,128)}, u32[]{:S(2)}) copy-start(s32[4,2]{0,1:T(2,128)} %param.18) | copy-start | bytes 100
  107.2 13.5 %all-to-all-start.3 = ((bf16[16,3,2048]{2,1,0:T(4,128)(2,1)}), bf16[16,3,2048]{2,1,0:T(4,128)(2,1)S(1)}, u32[]{:S(2)}, u32[]{:S(2)}) async-start(bf16[16,3,2048]{2,1,0:T(4,128)(2,1)} %copy.73), calls=%async_computation.3 | async-start | bytes 524288 | tf_op jit(solution)/shard_map/all_to_all | solution.py:104
where the time goes:
time: 123 us; the launch traced here: 122 us
  blocking collectives  55.2 us (45%)
  matrix products  22.1 us (18%)
  waiting for transfers between devices  21.7 us (18%)
  starting transfers between devices  10.5 us (9%)
  other arithmetic  7.51 us (6%)
  local copies, waits for them, and re-layouts  3.88 us (3%)
    all_gather x1, blocking collectives, local(): lax.all_gather(tokens, 'ep', axis=0, tiled=True)  24.2 us
    all_gather x1, blocking collectives, local(): lax.all_gather(mixed, 'ep', axis=0, tiled=True)  18.4 us
    all_to_all x1, blocking collectives, local(): lax.all_to_all(outgoing, 'ep', split_axis=0, concat_axis=0, tiled=True)  12.6 us
    all_to_all x1, waiting for transfers between devices, local(): lax.all_to_all(partial_rows.astype(jnp.bfloat16), 'ep', split_axis=0, con...  9.86 us
    dot_general x1, matrix products, local(): jnp.einsum('scf,fd->scd', hidden, expert_down, preferred_element_type=jnp...  7.88 us
    all_to_all x1, waiting for transfers between devices, local(): lax.all_to_all(mixer_cols, 'ep', split_axis=0, concat_axis=1, tiled=True)  6.45 us
    all_to_all x1, waiting for transfers between devices, local(): lax.all_to_all(projected, 'ep', split_axis=1, concat_axis=2, tiled=True)  5.34 us
    dot_general x1, matrix products, local(): jnp.einsum('scd,df->scf', arrived, expert_gate, preferred_element_type=jn...  4.49 us
  transfers between devices with their start and end apart: 3, of which 3 were waited for; matrix products, arithmetic and copies ran while one was open for 1% of the time, Pallas kernels for 0%

commit v1 on v0

--- a/solution.py
+++ b/solution.py
@@ -7,6 +7,12 @@
 EXPERTS = 4
 CAP = 3
 epsilon = 1e-06
+
+
+def tiled_gather(x, axis, dim):
+    devices = lax.axis_size(axis)
+    repeats = [devices if d == dim else 1 for d in range(x.ndim)]
+    return lax.all_to_all(jnp.tile(x, repeats), axis, split_axis=dim, concat_axis=dim, tiled=True)
 
 
 def rms_scale(values, gain):
@@ -59,7 +65,7 @@
     model_width = tokens.shape[1]
     expert_group = FF // expert_gate.shape[1]
     all_tokens, all_ids, all_weights = (
-        lax.all_gather(tokens, "ep", axis=0, tiled=True),
+        tiled_gather(tokens, "ep", 0),
         lax.all_gather(route_ids, "ep", axis=0, tiled=True),
         lax.all_gather(route_weights, "ep", axis=0, tiled=True),
     )

time: 123 us -> 118 us (0.959)
  blocking collectives: 55.2 us -> 31 us
  waiting for transfers between devices: 21.7 us -> 31.7 us
  starting transfers between devices: 10.5 us -> 17.9 us
  local copies, waits for them, and re-layouts: 3.88 us -> 5.55 us
    all_gather x1 -> x0, blocking collectives: 24.2 us -> none  [local(): lax.all_gather(tokens, 'ep', axis=0, tiled=True)]
    all_to_all x0 -> x1, waiting for transfers between devices: none -> 8.5 us  [tiled_gather(): lax.all_to_all(jnp.tile(x, repeats), axis, split_axis=dim, concat_axis=di...]
    all_to_all x0 -> x1, starting transfers between devices: none -> 7.41 us  [tiled_gather(): lax.all_to_all(jnp.tile(x, repeats), axis, split_axis=dim, concat_axis=di...]
    another operation x0 -> x1, local copies, waits for them, and re-layouts: none -> 1.58 us  [tiled_gather(): jnp.tile(x, repeats)]
    all_to_all x1, waiting for transfers between devices: 5.34 us -> 6.85 us  [local(): lax.all_to_all(projected, 'ep', split_axis=1, concat_axis=2, tiled=True)]
  transfers between devices with their start and end apart: 3 -> 4, of which waited for: 3 -> 4; matrix products, arithmetic and copies ran while one was open for 1% -> 1% of each run, Pallas kernels for 0% -> 0%
where the time goes in v1:
time: 118 us; the launch traced here: 117 us
  waiting for transfers between devices  31.7 us (27%)
  blocking collectives  31 us (26%)
  matrix products  22.1 us (19%)
  starting transfers between devices  17.9 us (15%)
  other arithmetic  7.58 us (6%)
  local copies, waits for them, and re-layouts  5.55 us (5%)
    all_gather x1, blocking collectives, local(): lax.all_gather(mixed, 'ep', axis=0, tiled=True)  18.4 us
    all_to_all x1, blocking collectives, local(): lax.all_to_all(outgoing, 'ep', split_axis=0, concat_axis=0, tiled=True)  12.6 us
    all_to_all x1, waiting for transfers between devices, local(): lax.all_to_all(partial_rows.astype(jnp.bfloat16), 'ep', split_axis=0, con...  9.86 us
    all_to_all x1, waiting for transfers between devices, tiled_gather(): lax.all_to_all(jnp.tile(x, repeats), axis, split_axis=dim, concat_axis=di...  8.5 us
    dot_general x1, matrix products, local(): jnp.einsum('scf,fd->scd', hidden, expert_down, preferred_element_type=jnp...  7.88 us
    all_to_all x1, starting transfers between devices, tiled_gather(): lax.all_to_all(jnp.tile(x, repeats), axis, split_axis=dim, concat_axis=di...  7.41 us
    all_to_all x1, waiting for transfers between devices, local(): lax.all_to_all(projected, 'ep', split_axis=1, concat_axis=2, tiled=True)  6.85 us
    all_to_all x1, waiting for transfers between devices, local(): lax.all_to_all(mixer_cols, 'ep', split_axis=0, concat_axis=1, tiled=True)  6.45 us
  transfers between devices with their start and end apart: 4, of which 4 were waited for; matrix products, arithmetic and copies ran while one was open for 1% of the time, Pallas kernels for 0%

profile of v1, /device:TPU:0, one launch (start us, length us, event | category | flops | bytes accessed | tf_op | source)
XLA Modules:
  0.0 116.8 jit_solution(5370064213257769578)
XLA Ops:
  0.6 1.6 %tile.2 = bf16[16,4,2048]{2,1,0:T(4,128)(2,1)} broadcast(bf16[4,2048]{1,0:T(4,128)(2,1)} %param.16), dimensions={1,2} | broadcast | bytes 278528 | tf_op jit(solution)/shard_map/tile | solution.py:15
  2.2 7.4 %all-to-all-start = ((bf16[16,4,2048]{2,1,0:T(4,128)(2,1)}), bf16[16,4,2048]{2,1,0:T(4,128)(2,1)S(1)}, u32[]{:S(2)}, u32[]{:S(2)}) async-start(bf16[16,4,2048]{2,1,0:T(4,128)(2,1)} %tile.2), calls=%async_computation | async-start | bytes 524288 | tf_op jit(solution)/shard_map/all_to_all | solution.py:15
  9.6 0.8 convert_reduce_fusion.1
  10.5 0.7 log_bitcast_fusion
  11.2 8.5 %all-to-all-done = bf16[16,4,2048]{2,1,0:T(4,128)(2,1)S(1)} async-done(((bf16[16,4,2048]{2,1,0:T(4,128)(2,1)}), bf16[16,4,2048]{2,1,0:T(4,128)(2,1)S(1)}, u32[]{:S(2)}, u32[]{:S(2)}) %all-to-all-start) | async-done | bytes 262176 | tf_op jit(solution)/shard_map/all_to_all | solution.py:15
  19.7 0.2 multiply_reduce_fusion
  20.0 0.8 multiply_convert_fusion
  20.9 0.2 fusion.17
  21.1 1.3 %fusion.18 = bf16[1,64,128]{2,1,0:T(8,128)(2,1)S(1)} fusion(bf16[64,2048]{1,0:T(8,128)(2,1)S(1)} %multiply_convert_fusion, bf16[2048,128]{1,0:T(8,128)(2,1)} %param.22), kind=kOutput, calls=%fused_computation.20 | convolution fusion | flops 33562624 | bytes 802816 | tf_op jit(solution)/shard_map/dot_general | solution.py:75
  22.4 1.3 %fusion.19 = bf16[1,64,128]{2,1,0:T(8,128)(2,1)S(1)} fusion(bf16[64,2048]{1,0:T(8,128)(2,1)S(1)} %multiply_convert_fusion, bf16[2048,128]{1,0:T(8,128)(2,1)} %param.23), kind=kOutput, calls=%fused_computation.21 | convolution fusion | flops 33562624 | bytes 802816 | tf_op jit(solution)/shard_map/dot_general | solution.py:75
  23.7 1.3 %fusion.20 = bf16[1,64,128]{2,1,0:T(8,128)(2,1)S(1)} fusion(bf16[64,2048]{1,0:T(8,128)(2,1)S(1)} %multiply_convert_fusion, bf16[2048,128]{1,0:T(8,128)(2,1)} %param.24), kind=kOutput, calls=%fused_computation.22 | convolution fusion | flops 33562624 | bytes 802816 | tf_op jit(solution)/shard_map/dot_general | solution.py:75
  25.0 0.7 copy.91
  25.7 3.5 %all-to-all-start.1 = ((bf16[4,64,128]{2,0,1:T(4,128)(2,1)}), bf16[4,64,128]{2,0,1:T(4,128)(2,1)S(1)}, u32[]{:S(2)}, u32[]{:S(2)}) async-start(bf16[4,64,128]{2,0,1:T(4,128)(2,1)} %copy.91), calls=%async_computation.1 | async-start | bytes 131072 | tf_op jit(solution)/shard_map/all_to_all | solution.py:79
  29.2 6.8 %all-to-all-done.1 = bf16[4,64,128]{2,0,1:T(4,128)(2,1)S(1)} async-done(((bf16[4,64,128]{2,0,1:T(4,128)(2,1)}), bf16[4,64,128]{2,0,1:T(4,128)(2,1)S(1)}, u32[]{:S(2)}, u32[]{:S(2)}) %all-to-all-start.1) | async-done | bytes 65568 | tf_op jit(solution)/shard_map/all_to_all | solution.py:79
  36.2 4.4 %multiply_add_fusion = f32[4,16,128,128]{3,2,1,0:T(8,128)S(1)} fusion(f32[4,16,128,128]{3,2,1,0:T(8,128)} %param.17, f32[4,16,128]{2,1,0:T(8,128)S(1)} %fusion.57, f32[4,16,128]{2,1,0:T(8,128)S(1)} %get-tuple-element.3, f32[4,16,128]{2,1,0:T(8,128)S(1)} %get-tuple-element.2), kind=kLoop, calls=%fused_computation.6 | loop fusion | flops 3145728 | bytes 8486912 | tf_op jit(solution)/shard_map/add | solution.py:37
  40.6 2.0 %copy-done.1 = f32[4,16,128,128]{3,2,1,0:T(8,128)} copy-done((f32[4,16,128,128]{3,2,1,0:T(8,128)}, f32[4,16,128,128]{3,2,1,0:T(8,128)S(1)}, u32[]{:S(2)}) %copy-start.1) | copy-done | bytes 4194328
  42.6 3.6 %fusion.73 = f32[4,16,1,128]{3,2,1,0:T(1,128)S(1)} fusion(f32[4,16,128,1]{2,3,1,0:T(1,128)S(1)} %bitcast.136, f32[4,16,128,128]{3,2,1,0:T(8,128)S(1)} %multiply_add_fusion), kind=kOutput, calls=%fused_computation.103 | convolution fusion | flops 12582912 | bytes 4259840 | tf_op jit(solution)/shard_map/thk,thkv->thv/dot_general | solution.py:40
  46.5 18.4 %all-gather = bf16[16,4,2048]{2,1,0:T(4,128)(2,1)S(1)} all-gather(bf16[1,4,2048]{2,1,0:T(4,128)(2,1)S(1)} %reshape.181), channel_id=1, replica_groups=mesh['grp'=2,'ep'=16] {'ep'}, dimensions={0}, use_global_device_ids=true | all-gather | bytes 278528 | tf_op jit(solution)/shard_map/all_gather | solution.py:82
  65.0 0.8 convolution_convert_fusion.1
  65.8 3.5 %all-to-all-start.2 = ((bf16[16,4,128]{2,1,0:T(4,128)(2,1)}), bf16[16,4,128]{2,1,0:T(4,128)(2,1)S(1)}, u32[]{:S(2)}, u32[]{:S(2)}) async-start(bf16[16,4,128]{2,1,0:T(4,128)(2,1)} %bitcast.20), calls=%async_computation.2 | async-start | bytes 32768 | tf_op jit(solution)/shard_map/all_to_all | solution.py:84
  69.3 6.5 %all-to-all-done.2 = bf16[16,4,128]{2,1,0:T(4,128)(2,1)S(1)} async-done(((bf16[16,4,128]{2,1,0:T(4,128)(2,1)}), bf16[16,4,128]{2,1,0:T(4,128)(2,1)S(1)}, u32[]{:S(2)}, u32[]{:S(2)}) %all-to-all-start.2) | async-done | bytes 16416 | tf_op jit(solution)/shard_map/all_to_all | solution.py:84
  75.8 0.1 multiply_reduce_fusion.1
  75.9 0.2 convolution_convert_fusion
  76.2 0.1 broadcast_in_dim.2
  76.3 12.6 %all_to_all.44 = bf16[16,3,2048]{2,1,0:T(4,128)(2,1)S(1)} all-to-all(bf16[16,3,2048]{2,1,0:T(4,128)(2,1)S(1)} %bitcast.129), channel_id=1, replica_groups=mesh['grp'=2,'ep'=16] {'ep'}, dimensions={0} | all-to-all | bytes 393216 | tf_op jit(solution)/shard_map/all_to_all | solution.py:103
  88.9 4.5 %fusion.4 = f32[16,3,1792]{2,0,1:T(8,128)S(1)} fusion(bf16[2048,1792]{1,0:T(8,128)(2,1)} %param.29, bf16[16,3,2048]{2,1,0:T(4,128)(2,1)S(1)} %all_to_all.44), kind=kOutput, calls=%fused_computation.4 | convolution fusion | flops 352321536 | bytes 7880704 | tf_op jit(solution)/shard_map/scd,df->scf/dot_general | solution.py:104
  93.4 7.9 %fusion.12 = bf16[16,3,2048]{2,0,1:T(8,128)(2,1)S(1)} fusion(bf16[1792,2048]{1,0:T(8,128)(2,1)} %param.31, bf16[2048,1792]{1,0:T(8,128)(2,1)} %param.30, f32[16,3,1792]{2,0,1:T(8,128)S(1)} %fusion.4, bf16[16,3,2048]{2,1,0:T(4,128)(2,1)S(1)} %all_to_all.44), kind=kOutput, calls=%fused_computation.9 | convolution fusion | flops 705257472 | bytes 15417344 | tf_op jit(solution)/shard_map/scf,fd->scd/dot_general | solution.py:107
  101.3 0.9 copy.98
  102.2 3.5 %all-to-all-start.4 = ((bf16[16,3,2048]{2,1,0:T(4,128)(2,1)}), bf16[16,3,2048]{2,1,0:T(4,128)(2,1)S(1)}, u32[]{:S(2)}, u32[]{:S(2)}) async-start(bf16[16,3,2048]{2,1,0:T(4,128)(2,1)} %copy.98), calls=%async_computation.4 | async-start | bytes 524288 | tf_op jit(solution)/shard_map/all_to_all | solution.py:110
  105.9 9.9 %all-to-all-done.4 = bf16[16,3,2048]{2,1,0:T(4,128)(2,1)S(1)} async-done(((bf16[16,3,2048]{2,1,0:T(4,128)(2,1)}), bf16[16,3,2048]{2,1,0:T(4,128)(2,1)S(1)}, u32[]{:S(2)}, u32[]{:S(2)}) %all-to-all-start.4) | async-done | bytes 196640 | tf_op jit(solution)/shard_map/all_to_all | solution.py:110
  115.7 0.1 convert_reduce_fusion
  115.8 0.9 fusion.16
  (34 shorter events, 0.7 us)
Async XLA Ops:
  0.6 20.2 %copy-start = (bf16[2048,128]{1,0:T(8,128)(2,1)S(1)}, bf16[2048,128]{1,0:T(8,128)(2,1)}, u32[]{:S(2)}) copy-start(bf16[2048,128]{1,0:T(8,128)(2,1)} %param.21) | copy-start | bytes 1572868
  2.2 17.4 %all-to-all-start = ((bf16[16,4,2048]{2,1,0:T(4,128)(2,1)}), bf16[16,4,2048]{2,1,0:T(4,128)(2,1)S(1)}, u32[]{:S(2)}, u32[]{:S(2)}) async-start(bf16[16,4,2048]{2,1,0:T(4,128)(2,1)} %tile.2), calls=%async_computation | async-start | bytes 524288 | tf_op jit(solution)/shard_map/all_to_all | solution.py:15
  23.7 22.7 %copy-start.5 = (f32[128]{0:T(128)S(1)}, f32[128]{0:T(128)}, u32[]{:S(2)}) copy-start(f32[128]{0:T(128)} %param.26) | copy-start | bytes 1540
  25.0 40.0 %copy-start.2 = (bf16[2048,128]{1,0:T(8,128)(2,1)S(1)}, bf16[2048,128]{1,0:T(8,128)(2,1)}, u32[]{:S(2)}) copy-start(bf16[2048,128]{1,0:T(8,128)(2,1)} %param.27) | copy-start | bytes 1572868
  25.7 10.4 %all-to-all-start.1 = ((bf16[4,64,128]{2,0,1:T(4,128)(2,1)}), bf16[4,64,128]{2,0,1:T(4,128)(2,1)S(1)}, u32[]{:S(2)}, u32[]{:S(2)}) async-start(bf16[4,64,128]{2,0,1:T(4,128)(2,1)} %copy.91), calls=%async_computation.1 | async-start | bytes 131072 | tf_op jit(solution)/shard_map/all_to_all | solution.py:79
  36.1 39.7 %copy-start.3 = (bf16[4,2048]{1,0:T(4,128)(2,1)S(1)}, bf16[4,2048]{1,0:T(4,128)(2,1)}, u32[]{:S(2)}) copy-start(bf16[4,2048]{1,0:T(4,128)(2,1)} %param.16) | copy-start | bytes 49156
  36.1 39.8 %copy-start.6 = (f32[2048]{0:T(1024)S(1)}, f32[2048]{0:T(1024)}, u32[]{:S(2)}) copy-start(f32[2048]{0:T(1024)} %param.28) | copy-start | bytes 24580
  40.6 2.0 %copy-start.1 = (f32[4,16,128,128]{3,2,1,0:T(8,128)}, f32[4,16,128,128]{3,2,1,0:T(8,128)S(1)}, u32[]{:S(2)}) copy-start(f32[4,16,128,128]{3,2,1,0:T(8,128)S(1)} %multiply_add_fusion) | copy-start | bytes 12582916
  65.8 10.0 %all-to-all-start.2 = ((bf16[16,4,128]{2,1,0:T(4,128)(2,1)}), bf16[16,4,128]{2,1,0:T(4,128)(2,1)S(1)}, u32[]{:S(2)}, u32[]{:S(2)}) async-start(bf16[16,4,128]{2,1,0:T(4,128)(2,1)} %bitcast.20), calls=%async_computation.2 | async-start | bytes 32768 | tf_op jit(solution)/shard_map/all_to_all | solution.py:84
  93.4 12.3 %copy-start.7 = (bf16[4,2]{0,1:T(2,128)(2,1)S(1)}, bf16[4,2]{0,1:T(2,128)(2,1)}, u32[]{:S(2)}) copy-start(bf16[4,2]{0,1:T(2,128)(2,1)} %param.19) | copy-start | bytes 52
  93.4 12.3 %copy-start.4 = (s32[4,2]{0,1:T(2,128)S(1)}, s32[4,2]{0,1:T(2,128)}, u32[]{:S(2)}) copy-start(s32[4,2]{0,1:T(2,128)} %param.18) | copy-start | bytes 100
  102.2 13.5 %all-to-all-start.4 = ((bf16[16,3,2048]{2,1,0:T(4,128)(2,1)}), bf16[16,3,2048]{2,1,0:T(4,128)(2,1)S(1)}, u32[]{:S(2)}, u32[]{:S(2)}) async-start(bf16[16,3,2048]{2,1,0:T(4,128)(2,1)} %copy.98), calls=%async_computation.4 | async-start | bytes 524288 | tf_op jit(solution)/shard_map/all_to_all | solution.py:110
